TPU v7x, 1024 devices: a whole 4x8x16 slice. The times are simulated.
1024 devices in a mesh: sp: 16 (over z), dp: 64 (over y, x, core).
Axes of the slice: x: 4, y: 8, z: 16, core: 2. Of those that a mesh axis runs over, the one named last changes fastest.
Arguments:
- queries: bfloat16 [64, 2048, 1024], P('dp', 'sp'), may hold values from -6 to 6
- key_rows: bfloat16 [64, 2048, 1024], P('dp', 'sp'), may hold values from -6 to 6
- values: bfloat16 [64, 2048, 2048], P('dp', 'sp'), may hold values from -6 to 6
- out_gate: bfloat16 [64, 2048, 2048], P('dp', 'sp'), may hold values from -6 to 6
- input_gate: bfloat16 [64, 4, 2048], P('dp', None, 'sp'), may hold values from -6 to 205
- forget_gate: bfloat16 [64, 4, 2048], P('dp', None, 'sp'), may hold values from 0.5 to 13
- out_weight: bfloat16 [2048, 2048], P(None, 'dp'), may hold values from -0.125 to 0.125
Outputs:
- layer_out: bfloat16 [64, 2048, 2048], P('dp', 'sp')
All inputs are finite; a program needn't handle non-finite values.
Results may differ from a plain program's by a relative error of at most 0.0057.
Values may be sent and summed in bfloat16 or wider, within the bound.
A program may use at most 64 MiB of HBM per device.

v0:
```python
import math

import jax
import jax.numpy as jnp
from jax import lax
from jax.sharding import PartitionSpec as P

BLOCK = 128


def in_one_piece(arrays, axis, split_dim, concat_dim, along):
    widths = [math.prod(a.shape[along:]) for a in arrays]
    both = jnp.concatenate(
        [a.reshape(*a.shape[:along], w) for a, w in zip(arrays, widths)], axis=along
    )
    result = lax.all_to_all(both, axis, split_axis=split_dim, concat_axis=concat_dim, tiled=True)
    parts = jnp.split(result, [sum(widths[:k]) for k in range(1, len(widths))], axis=along)
    return tuple(
        (b.reshape(*result.shape[:along], *a.shape[along:]) for a, b in zip(arrays, parts))
    )


def memory_cell(query_rows, key_in, value_rows, input_log, forget_log):
    block_count = query_rows.shape[0] // BLOCK
    key_width = query_rows.shape[1]
    value_width = value_rows.shape[1]
    key_scale = key_width ** (-0.5)
    causal = lax.broadcasted_iota(jnp.int32, (BLOCK, BLOCK), 0) >= lax.broadcasted_iota(
        jnp.int32, (BLOCK, BLOCK), 1
    )
    highest = lax.Precision.HIGHEST

    def block_step(state_in, inputs):
        memory, normer, stabil = state_in
        query_part, key_part, value_part, gain_part, decay_part = inputs
        query_part = query_part.astype(jnp.float32)
        key_part = key_part.astype(jnp.float32) * key_scale
        value_part = value_part.astype(jnp.float32)
        running = jnp.cumsum(decay_part)
        log_weight = running[:, None] - running[None, :] + gain_part[None, :]
        log_weight = jnp.where(causal, log_weight, -jnp.inf)
        carried_log = running + stabil
        row_top = jnp.maximum(carried_log, jnp.max(log_weight, axis=1))
        scores = jnp.dot(query_part, key_part.T, precision=highest) * jnp.exp(
            log_weight - row_top[:, None]
        )
        carried = jnp.exp(carried_log - row_top)
        numerator = jnp.dot(scores, value_part, precision=highest) + carried[:, None] * jnp.dot(
            query_part, memory, precision=highest
        )
        denominator = jnp.sum(scores, axis=1) + carried * jnp.dot(
            query_part, normer, precision=highest
        )
        output = numerator / jnp.maximum(jnp.abs(denominator), 1.0)[:, None]
        block_end = running[-1]
        weight_log = block_end - running + gain_part
        new_top = jnp.maximum(block_end + stabil, jnp.max(weight_log))
        weights = jnp.exp(weight_log - new_top)
        retain = jnp.exp(block_end + stabil - new_top)
        memory = retain * memory + jnp.dot(
            (key_part * weights[:, None]).T, value_part, precision=highest
        )
        normer = retain * normer + jnp.dot(weights, key_part, precision=highest)
        return ((memory, normer, new_top), output)

    start_state = (
        jnp.zeros((key_width, value_width), jnp.float32),
        jnp.zeros((key_width,), jnp.float32),
        jnp.zeros((), jnp.float32),
    )
    blocks = tuple(
        (
            source.reshape((block_count, BLOCK) + source.shape[1:])
            for source in (query_rows, key_in, value_rows, input_log, forget_log)
        )
    )
    _, outputs = lax.scan(block_step, start_state, blocks)
    return outputs.reshape(block_count * BLOCK, value_width)


def body(queries, key_rows, values, out_gate, input_gate, forget_gate, out_weight):
    group_count = lax.axis_size("sp")
    token_count = queries.shape[1]
    head_count = input_gate.shape[1]
    copies = group_count // head_count
    head_key = queries.shape[2] // head_count
    slice_width = values.shape[2] // group_count
    whole_weight = lax.all_gather(out_weight, "dp", axis=1, tiled=True)

    def spread(source):
        widened = jnp.broadcast_to(
            source[0].reshape(token_count, head_count, 1, head_key),
            (token_count, head_count, copies, head_key),
        )
        return widened.reshape(token_count, group_count, head_key)

    def spread_gate(source):
        return jnp.repeat(source[0].T, copies, axis=1)

    query_all, key_all = (
        lax.all_to_all(spread(queries), "sp", split_axis=1, concat_axis=0, tiled=True),
        lax.all_to_all(spread(key_rows), "sp", split_axis=1, concat_axis=0, tiled=True),
    )
    value_all, input_all, forget_all = in_one_piece(
        (
            values[0].reshape(token_count, group_count, slice_width),
            spread_gate(input_gate),
            spread_gate(forget_gate),
        ),
        "sp",
        1,
        0,
        2,
    )
    output = memory_cell(
        query_all[:, 0],
        key_all[:, 0],
        value_all[:, 0],
        input_all[:, 0].astype(jnp.float32),
        jax.nn.log_sigmoid(forget_all[:, 0].astype(jnp.float32)),
    )
    hidden = output.astype(jnp.bfloat16)
    token_rows = lax.all_to_all(hidden, "sp", split_axis=0, concat_axis=1, tiled=True)
    gated_rows = (
        token_rows.astype(jnp.float32) * jax.nn.sigmoid(out_gate[0].astype(jnp.float32))
    ).astype(jnp.bfloat16)
    projected = jnp.dot(gated_rows, whole_weight, preferred_element_type=jnp.float32)
    return projected.astype(jnp.bfloat16)[None]


def solution(mesh):
    return jax.shard_map(
        body,
        mesh=mesh,
        in_specs=(
            P("dp", "sp", None),
            P("dp", "sp", None),
            P("dp", "sp", None),
            P("dp", "sp", None),
            P("dp", None, "sp"),
            P("dp", None, "sp"),
            P(None, "dp"),
        ),
        out_specs=P("dp", "sp", None),
        check_vma=False,
    )
```

profile of v0, /device:TPU:6, one launch (start us, length us, event | category | flops | bytes accessed | tf_op | source)
XLA Modules:
  0.0 364.1 jit_solution(2566961490169957024)
XLA Ops:
  6.5 1.3 copy.33
  10.1 18.9 %all-to-all-start = ((bf16[128,16,130]{0,2,1:T(8,128)(2,1)}), bf16[128,16,130]{0,2,1:T(8,128)(2,1)S(1)}, u32[]{:S(2)}, u32[]{:S(2)}) async-start(bf16[128,16,130]{0,2,1:T(8,128)(2,1)} %pad_maximum_fusion), calls=%async_computation | async-start | bytes 1114112 | tf_op jit(solution)/shard_map/all_to_all | solution.py:16
  29.2 29.7 %all-to-all-done = bf16[128,16,130]{0,2,1:T(8,128)(2,1)S(1)} async-done(((bf16[128,16,130]{0,2,1:T(8,128)(2,1)}), bf16[128,16,130]{0,2,1:T(8,128)(2,1)S(1)}, u32[]{:S(2)}, u32[]{:S(2)}) %all-to-all-start) | async-done | bytes 532512 | tf_op jit(solution)/shard_map/all_to_all | solution.py:16
  60.0 7.0 %all-to-all-start.1 = ((bf16[128,16,256]{2,0,1:T(8,128)(2,1)}), bf16[128,16,256]{2,0,1:T(8,128)(2,1)S(1)}, u32[]{:S(2)}, u32[]{:S(2)}) async-start(bf16[128,16,256]{2,0,1:T(8,128)(2,1)} %bitcast.11), calls=%async_computation.1 | async-start | bytes 2097152 | tf_op jit(solution)/shard_map/all_to_all | solution.py:102
  67.2 49.8 %all-to-all-done.1 = bf16[128,16,256]{2,0,1:T(8,128)(2,1)S(1)} async-done(((bf16[128,16,256]{2,0,1:T(8,128)(2,1)}), bf16[128,16,256]{2,0,1:T(8,128)(2,1)S(1)}, u32[]{:S(2)}, u32[]{:S(2)}) %all-to-all-start.1) | async-done | bytes 1048608 | tf_op jit(solution)/shard_map/all_to_all | solution.py:102
  118.1 7.9 %all-to-all-start.2 = ((bf16[128,16,256]{2,0,1:T(8,128)(2,1)}), bf16[128,16,256]{2,0,1:T(8,128)(2,1)S(1)}, u32[]{:S(2)}, u32[]{:S(2)}) async-start(bf16[128,16,256]{2,0,1:T(8,128)(2,1)} %bitcast.16), calls=%async_computation.2 | async-start | bytes 2097152 | tf_op jit(solution)/shard_map/all_to_all | solution.py:101
  128.3 47.9 %all-to-all-done.2 = bf16[128,16,256]{2,0,1:T(8,128)(2,1)S(1)} async-done(((bf16[128,16,256]{2,0,1:T(8,128)(2,1)}), bf16[128,16,256]{2,0,1:T(8,128)(2,1)S(1)}, u32[]{:S(2)}, u32[]{:S(2)}) %all-to-all-start.2) | async-done | bytes 1048608 | tf_op jit(solution)/shard_map/all_to_all | solution.py:101
  176.2 136.3 %while.17 = (s32[]{:T(128)}, f32[256,128]{1,0:T(8,128)S(1)}, f32[256]{0:T(256)S(1)}, f32[]{:T(128)}, bf16[16,128,128]{1,2,0:T(8,128)(2,1)}, /*index=5*/f32[16,12...) while((s32[]{:T(128)}, f32[256,128]{1,0:T(8,128)S(1)}, ...), condition=%wide.region_5.6_spmd.clone, body=%wide.region_0.5_spmd.clone.sunk | while | flops 177555968 | bytes 1306361 | solution.py:77
  177.7 1.2 fusion.92
  186.3 1.2 fusion.92
  194.8 1.2 fusion.92
  203.3 1.2 fusion.92
  211.8 1.2 fusion.92
  220.3 1.2 fusion.92
  228.9 1.2 fusion.92
  237.4 1.2 fusion.92
  245.9 1.2 fusion.92
  254.4 1.2 fusion.92
  262.9 1.2 fusion.92
  271.5 1.2 fusion.92
  280.0 1.2 fusion.92
  312.5 8.1 %all-to-all-start.3 = ((bf16[16,128,128]{1,2,0:T(8,128)(2,1)}), bf16[16,128,128]{1,2,0:T(8,128)(2,1)S(1)}, u32[]{:S(2)}, u32[]{:S(2)}) async-start(bf16[16,128,128]{1,2,0:T(8,128)(2,1)} %get-tuple-element.62), calls=%async_computation.3 | async-start | bytes 1048576 | tf_op jit(solution)/shard_map/all_to_all | solution.py:123
  320.9 28.9 %all-to-all-done.3 = bf16[16,128,128]{1,2,0:T(8,128)(2,1)S(1)} async-done(((bf16[16,128,128]{1,2,0:T(8,128)(2,1)}), bf16[16,128,128]{1,2,0:T(8,128)(2,1)S(1)}, u32[]{:S(2)}, u32[]{:S(2)}) %all-to-all-start.3) | async-done | bytes 524320 | tf_op jit(solution)/shard_map/all_to_all | solution.py:123
  350.2 7.1 %fusion.53 = bf16[1,128,2048]{2,1,0:T(8,128)(2,1)} fusion(bf16[128,2048]{0,1:T(8,128)(2,1)S(1)} %fusion.54, bf16[2048,2048]{0,1:T(8,128)(2,1)} %all-gather.2.cloned.1.call-done), kind=kOutput, calls=%fused_computation.68 | convolution fusion | flops 1074003968 | bytes 9437184 | tf_op jit(solution)/shard_map/dot_general | solution.py:127
  (291 shorter events, 107.5 us)
Async XLA Ops:
  9.2 19.7 %copy-start.1 = (bf16[1,128,1024]{2,1,0:T(8,128)(2,1)S(1)}, bf16[1,128,1024]{2,1,0:T(8,128)(2,1)}, u32[]{:S(2)}) copy-start(bf16[1,128,1024]{2,1,0:T(8,128)(2,1)} %param.10) | copy-start | bytes 786436
  10.1 48.8 %all-to-all-start = ((bf16[128,16,130]{0,2,1:T(8,128)(2,1)}), bf16[128,16,130]{0,2,1:T(8,128)(2,1)S(1)}, u32[]{:S(2)}, u32[]{:S(2)}) async-start(bf16[128,16,130]{0,2,1:T(8,128)(2,1)} %pad_maximum_fusion), calls=%async_computation | async-start | bytes 1114112 | tf_op jit(solution)/shard_map/all_to_all | solution.py:16
  60.0 7.0 %copy-start.2 = (bf16[1,128,1024]{2,1,0:T(8,128)(2,1)S(1)}, bf16[1,128,1024]{2,1,0:T(8,128)(2,1)}, u32[]{:S(2)}) copy-start(bf16[1,128,1024]{2,1,0:T(8,128)(2,1)} %param.9) | copy-start | bytes 786436
  60.0 57.0 %all-to-all-start.1 = ((bf16[128,16,256]{2,0,1:T(8,128)(2,1)}), bf16[128,16,256]{2,0,1:T(8,128)(2,1)S(1)}, u32[]{:S(2)}, u32[]{:S(2)}) async-start(bf16[128,16,256]{2,0,1:T(8,128)(2,1)} %bitcast.11), calls=%async_computation.1 | async-start | bytes 2097152 | tf_op jit(solution)/shard_map/all_to_all | solution.py:102
  118.1 58.0 %all-to-all-start.2 = ((bf16[128,16,256]{2,0,1:T(8,128)(2,1)}), bf16[128,16,256]{2,0,1:T(8,128)(2,1)S(1)}, u32[]{:S(2)}, u32[]{:S(2)}) async-start(bf16[128,16,256]{2,0,1:T(8,128)(2,1)} %bitcast.16), calls=%async_computation.2 | async-start | bytes 2097152 | tf_op jit(solution)/shard_map/all_to_all | solution.py:101
  126.1 224.1 %all-gather.2.cloned.1.call-start = ((), (), s32[]{:S(2)}) async-start(), calls=%async_computation.4 | async-start | bytes 8519680 | tf_op jit(solution)/shard_map/all_gather | solution.py:88
  312.5 8.1 %copy-start = (bf16[1,128,2048]{2,1,0:T(8,128)(2,1)S(1)}, bf16[1,128,2048]{2,1,0:T(8,128)(2,1)}, u32[]{:S(2)}) copy-start(bf16[1,128,2048]{2,1,0:T(8,128)(2,1)} %param.12) | copy-start | bytes 1572868
  312.5 37.3 %all-to-all-start.3 = ((bf16[16,128,128]{1,2,0:T(8,128)(2,1)}), bf16[16,128,128]{1,2,0:T(8,128)(2,1)S(1)}, u32[]{:S(2)}, u32[]{:S(2)}) async-start(bf16[16,128,128]{1,2,0:T(8,128)(2,1)} %get-tuple-element.62), calls=%async_computation.3 | async-start | bytes 1048576 | tf_op jit(solution)/shard_map/all_to_all | solution.py:123
Sparse Core Ops, SparseCore 0:
  131.4 97.9 all-gather.1
where the time goes:
time: 368 us; the launch traced here: 364 us
  waiting for transfers between devices  157 us (43%)
  matrix products  54.7 us (15%)
  other arithmetic  46.9 us (13%)
  starting transfers between devices  41.9 us (11%)
  local copies, waits for them, and re-layouts  29.2 us (8%)
  loops' own time  20.8 us (6%)
  between operations  13.6 us (4%)
    all_to_all x1, waiting for transfers between devices, body(): lax.all_to_all(spread(key_rows), 'sp', split_axis=1, concat_axis=0, tiled...  49.8 us
    all_to_all x1, waiting for transfers between devices, body(): lax.all_to_all(spread(queries), 'sp', split_axis=1, concat_axis=0, tiled=...  47.9 us
    all_to_all x1, waiting for transfers between devices, in_one_piece(): lax.all_to_all(both, axis, split_axis=split_dim, concat_axis=concat_dim,...  29.7 us
    all_to_all x1, waiting for transfers between devices, body(): lax.all_to_all(hidden, 'sp', split_axis=0, concat_axis=1, tiled=True)  28.9 us
    another operation x1, loops' own time, memory_cell(): _, outputs = lax.scan(block_step, start_state, blocks)  20.8 us
    reduce_max x16, other arithmetic, block_step(): new_top = jnp.maximum(block_end + stabil, jnp.max(weight_log))  19.2 us
    all_to_all x1, starting transfers between devices, in_one_piece(): lax.all_to_all(both, axis, split_axis=split_dim, concat_axis=concat_dim,...  18.9 us
    dot_general x16, matrix products, block_step(): jnp.dot((key_part * weights[:, None]).T, value_part, precision=highest)  17.8 us
  transfers between devices with their start and end apart: 5, of which 4 were waited for; matrix products, arithmetic and copies ran while one was open for 32% of the time, Pallas kernels for 0%

commit v1 on v0

v1 whole, which is shorter than its diff:
```python
import functools

import jax
import jax.numpy as jnp
from jax import lax
from jax.experimental import pallas as pl
from jax.experimental.pallas import tpu as pltpu
from jax.sharding import PartitionSpec as P

MESH = pl.DeviceIdType.MESH
HEADS = 4
DK = 256
DV = 512
T = 128
ROWS = 16
PIECES = DK // ROWS
F32 = jnp.float32
BF16 = jnp.bfloat16


def local_terms(h, q_ref, k_ref, v_ref, run, gain, part, norm_loc, top_loc, cm_scr, kcol_scr):
    row = lax.broadcasted_iota(jnp.int32, (T, T), 0)
    col = lax.broadcasted_iota(jnp.int32, (T, T), 1)
    d = gain[h : h + 1, :] - run[h : h + 1, :]
    dd = jnp.broadcast_to(d, (T, T))
    running_top = jnp.max(jnp.where(col <= row, dd, -jnp.inf), axis=1, keepdims=True)
    d_col = jnp.sum(jnp.where(col == row, dd, 0.0), axis=1, keepdims=True)
    top = jnp.max(d, axis=1, keepdims=True)
    cm_scr[h] = jnp.broadcast_to(running_top, (T, T))
    top_loc[h : h + 1, :] = jnp.broadcast_to(top, (1, DK))
    keys = k_ref[:, h * DK : (h + 1) * DK].astype(F32) * (DK**-0.5)
    weighted = keys * jnp.exp(d_col - top)
    norm_loc[h : h + 1, :] = jnp.sum(weighted, axis=0, keepdims=True)
    state = lax.dot_general(
        weighted.astype(BF16),
        v_ref[:, h * DV : (h + 1) * DV],
        (((0,), (0,)), ((), ())),
        preferred_element_type=F32,
    )
    part[h * PIECES : (h + 1) * PIECES] = state.reshape(PIECES, ROWS, DV)


def within_block(h, q_ref, k_ref, v_ref, run, gain, cm_scr, sv_scr, den_scr):
    row = lax.broadcasted_iota(jnp.int32, (T, T), 0)
    col = lax.broadcasted_iota(jnp.int32, (T, T), 1)
    d = gain[h : h + 1, :] - run[h : h + 1, :]
    weight = jnp.where(col <= row, jnp.exp(jnp.minimum(d - cm_scr[h], 0.0)), 0.0)
    raw = lax.dot_general(
        q_ref[:, h * DK : (h + 1) * DK],
        k_ref[:, h * DK : (h + 1) * DK],
        (((1,), (1,)), ((), ())),
        preferred_element_type=F32,
    )
    scores = raw * (DK**-0.5) * weight
    den_scr[h] = jnp.broadcast_to(jnp.sum(scores, axis=1, keepdims=True), (T, T))
    high = scores.astype(BF16)
    low = (scores - high.astype(F32)).astype(BF16)
    values = v_ref[:, h * DV : (h + 1) * DV]
    sv_scr[h] = jnp.dot(high, values, preferred_element_type=F32) + jnp.dot(
        low, values, preferred_element_type=F32
    )


def cell_kernel(
    q_ref,
    k_ref,
    v_ref,
    og_ref,
    ig_ref,
    fg_ref,
    out_ref,
    part,
    recv,
    send,
    head_in,
    head_out,
    norm_loc,
    top_loc,
    end_loc,
    keep_scr,
    add_scr,
    cm_scr,
    den_scr,
    sv_scr,
    gate_scr,
    send_sem,
    recv_sem,
):
    me = lax.axis_index("sp")
    size = lax.axis_size("sp")
    right = lax.rem(me + 1, size)
    left = lax.rem(me + size - 1, size)

    barrier = pltpu.get_barrier_semaphore()
    for other in (left, right):
        pl.semaphore_signal(barrier, inc=1, device_id={"sp": other}, device_id_type=MESH)

    def piece_copy(i):
        return pltpu.make_async_remote_copy(
            src_ref=send.at[i],
            dst_ref=recv.at[i],
            send_sem=send_sem.at[i],
            recv_sem=recv_sem.at[i],
            device_id={"sp": right},
            device_id_type=MESH,
        )

    last = HEADS * PIECES
    head_copy = pltpu.make_async_remote_copy(
        src_ref=head_out,
        dst_ref=head_in,
        send_sem=send_sem.at[last],
        recv_sem=recv_sem.at[last],
        device_id={"sp": right},
        device_id_type=MESH,
    )

    gain = ig_ref[...].astype(F32)
    decay = -jnp.log1p(jnp.exp(-fg_ref[...].astype(F32)))
    row = lax.broadcasted_iota(jnp.int32, (T, T), 0)
    col = lax.broadcasted_iota(jnp.int32, (T, T), 1)
    upto = jnp.where(row <= col, 1.0, 0.0).astype(F32)
    run = jnp.dot(decay, upto, precision=lax.Precision.HIGHEST, preferred_element_type=F32)
    end_loc[...] = jnp.broadcast_to(run[:, T - 1 : T], (HEADS, DK))
    for h in range(HEADS):
        local_terms(h, q_ref, k_ref, v_ref, run, gain, part, norm_loc, top_loc, cm_scr, None)

    pl.semaphore_wait(barrier, 2)

    def step_header(stab, norm):
        new = jnp.maximum(stab, top_loc[...])
        keep = jnp.exp(stab - new)
        add = jnp.exp(top_loc[...] - new)
        head_out[0:HEADS, :] = end_loc[...] + new
        head_out[HEADS:, :] = keep * norm + add * norm_loc[...]
        keep_scr[...] = jnp.concatenate([keep, keep], axis=1)
        add_scr[...] = jnp.concatenate([add, add], axis=1)

    @pl.when(me == 0)
    def _():
        head_in[...] = jnp.zeros((2 * HEADS, DK), F32)
        step_header(jnp.zeros((HEADS, DK), F32), jnp.zeros((HEADS, DK), F32))
        head_copy.start()
        for h in range(HEADS):

            def first(i, _, h=h):
                at = h * PIECES + i
                send[at] = (add_scr[h : h + 1, :] * part[at]).astype(BF16)
                piece_copy(at).start()
                return 0

            lax.fori_loop(0, PIECES, first, 0)

        def clear(i, _):
            recv[i] = jnp.zeros((ROWS, DV), BF16)
            return 0

        lax.fori_loop(0, last, clear, 0)

    for h in range(HEADS):
        within_block(h, q_ref, k_ref, v_ref, run, gain, cm_scr, sv_scr, den_scr)
        gate_scr[:, h * DV : (h + 1) * DV] = jax.nn.sigmoid(
            og_ref[:, h * DV : (h + 1) * DV].astype(F32)
        )

    def consume(h):
        q = q_ref[:, h * DK : (h + 1) * DK]
        stab = head_in[h : h + 1, 0:T]
        norm = head_in[HEADS + h : HEADS + h + 1, :]
        top = jnp.maximum(stab, cm_scr[h])
        own = jnp.exp(cm_scr[h] - top)
        old = jnp.exp(stab - top)
        past = jnp.sum(q.astype(F32) * norm, axis=1, keepdims=True)
        den = own * den_scr[h] + old * past
        inv = 1.0 / jnp.maximum(jnp.abs(den), 1.0)
        own = own * inv
        old = old * inv
        state = recv[h * PIECES : (h + 1) * PIECES].reshape(DK, DV)
        carried = jnp.dot(q, state, preferred_element_type=F32)
        for c in range(DV // T):
            at = slice(c * T, (c + 1) * T)
            cell = own * sv_scr[h, :, at] + old * carried[:, at]
            hidden = cell.astype(BF16).astype(F32)
            cols = slice(h * DV + c * T, h * DV + (c + 1) * T)
            out_ref[:, cols] = (hidden * gate_scr[:, cols]).astype(BF16)

    @pl.when(jnp.logical_and(me > 0, me < size - 1))
    def _():
        head_copy.wait_recv()
        step_header(head_in[0:HEADS, :], head_in[HEADS:, :])
        head_copy.start()
        for h in range(HEADS):

            def middle(i, _, h=h):
                at = h * PIECES + i
                piece_copy(at).wait_recv()
                new = keep_scr[h : h + 1, :] * recv[at].astype(F32) + add_scr[h : h + 1, :] * part[at]
                send[at] = new.astype(BF16)
                piece_copy(at).start()
                return 0

            lax.fori_loop(0, PIECES, middle, 0)

    @pl.when(me == size - 1)
    def _():
        head_copy.wait_recv()

    for h in range(HEADS):

        @pl.when(me == size - 1)
        def _(h=h):
            def final(i, _):
                piece_copy(h * PIECES + i).wait_recv()
                return 0

            lax.fori_loop(0, PIECES, final, 0)

        consume(h)

    @pl.when(me < size - 1)
    def _():
        head_copy.wait_send()

        def drain(i, _):
            piece_copy(i).wait_send()
            return 0

        lax.fori_loop(0, last, drain, 0)


def cell(q, k, v, og, ig, fg):
    pieces = HEADS * PIECES
    return pl.pallas_call(
        cell_kernel,
        out_shape=jax.ShapeDtypeStruct((T, HEADS * DV), BF16),
        in_specs=[pl.BlockSpec(memory_space=pltpu.VMEM)] * 6,
        out_specs=pl.BlockSpec(memory_space=pltpu.VMEM),
        scratch_shapes=[
            pltpu.VMEM((pieces, ROWS, DV), F32),
            pltpu.VMEM((pieces, ROWS, DV), BF16),
            pltpu.VMEM((pieces, ROWS, DV), BF16),
            pltpu.VMEM((2 * HEADS, DK), F32),
            pltpu.VMEM((2 * HEADS, DK), F32),
            pltpu.VMEM((HEADS, DK), F32),
            pltpu.VMEM((HEADS, DK), F32),
            pltpu.VMEM((HEADS, DK), F32),
            pltpu.VMEM((HEADS, DV), F32),
            pltpu.VMEM((HEADS, DV), F32),
            pltpu.VMEM((HEADS, T, T), F32),
            pltpu.VMEM((HEADS, T, T), F32),
            pltpu.VMEM((HEADS, T, DV), F32),
            pltpu.VMEM((T, HEADS * DV), F32),
            pltpu.SemaphoreType.DMA((pieces + 1,)),
            pltpu.SemaphoreType.DMA((pieces + 1,)),
        ],
        compiler_params=pltpu.CompilerParams(collective_id=0, has_side_effects=True),
        cost_estimate=pl.CostEstimate(flops=10**11, bytes_accessed=2 * 10**7, transcendentals=0),
    )(q, k, v, og, ig, fg)


def body(queries, key_rows, values, out_gate, input_gate, forget_gate, out_weight):
    whole_weight = lax.all_gather(out_weight, "dp", axis=1, tiled=True)
    gated = cell(
        queries[0], key_rows[0], values[0], out_gate[0], input_gate[0], forget_gate[0]
    )
    projected = jnp.dot(gated, whole_weight, preferred_element_type=F32)
    return projected.astype(BF16)[None]


def solution(mesh):
    return jax.shard_map(
        body,
        mesh=mesh,
        in_specs=(
            P("dp", "sp", None),
            P("dp", "sp", None),
            P("dp", "sp", None),
            P("dp", "sp", None),
            P("dp", None, "sp"),
            P("dp", None, "sp"),
            P(None, "dp"),
        ),
        out_specs=P("dp", "sp", None),
        check_vma=False,
    )
```

time: 368 us -> 134 us (0.36)
  the two profiles are of different devices: /device:TPU:6 before, /device:TPU:1 now
where the time goes in v1:
time: 134 us
  waiting for transfers between devices  70.4 us (53%)
  Pallas kernels  43 us (32%)
  between operations  13.4 us (10%)
  matrix products  7.25 us (5%)
    all_gather x1, waiting for transfers between devices, body(): whole_weight = lax.all_gather(out_weight, 'dp', axis=1, tiled=True)  69.7 us
    pallas_call x1, Pallas kernels, cell(): pl.pallas_call(cell_kernel, out_shape=jax.ShapeDtypeStruct((T, HEADS * DV...  43 us
    dot_general x1, matrix products, body(): projected = jnp.dot(gated, whole_weight, preferred_element_type=F32)  7.25 us
  transfers between devices with their start and end apart: 1, of which 1 were waited for; matrix products, arithmetic and copies ran while one was open for 0% of the time, Pallas kernels for 32%

profile of v1, /device:TPU:1, one launch (start us, length us, event | category | flops | bytes accessed | tf_op | source)
XLA Modules:
  0.0 134.0 jit_solution(8868009853097086664)
XLA Ops:
  6.5 0.0 all-gather.2.cloned.1.call-start
  6.5 0.7 all-gather.2.cloned.1.call-update
  7.3 43.0 %shard_map.73 = bf16[128,2048]{1,0:T(8,128)(2,1)} custom-call(bf16[128,1024]{1,0:T(8,128)(2,1)} %bitcast.12, bf16[128,1024]{1,0:T(8,128)(2,1)} %bitcast.13, bf16[128,2048]{1,0:T(8,128)(2,1)} %bitcast.10, bf16[128,2048]{1,0:T(8,128)(2,1)} %bitcast.11, bf16[4,128]{1,0:T(4,128)(2,1)} %bitcast.14, bf16[4,128]{1,0:T(4,128)(2,1)} %bitcast.15), custom_call_target="tpu_custom_call" | custom-call | flops 99999997952 | bytes 20000000 | tf_op jit(solution)/shard_map/pallas_call | solution.py:233
  50.2 69.7 %all-gather.2.cloned.1.call-done = bf16[2048,2048]{0,1:T(8,128)(2,1)} async-done(((bf16[2048,32]{0,1:T(8,128)(2,1)}), bf16[2048,2048]{0,1:T(8,128)(2,1)}) %all-gather.2.cloned.1.call-update) | async-done | bytes 8388624 | tf_op jit(solution)/shard_map/all_gather | solution.py:262
  119.9 7.3 %fusion = bf16[1,128,2048]{2,1,0:T(8,128)(2,1)} fusion(bf16[128,2048]{1,0:T(8,128)(2,1)} %shard_map.73, bf16[2048,2048]{0,1:T(8,128)(2,1)} %all-gather.2.cloned.1.call-done), kind=kOutput, calls=%fused_computation.1 | convolution fusion | flops 1074003968 | bytes 9437184 | tf_op jit(solution)/shard_map/dot_general | solution.py:266
Async XLA Ops:
  6.5 113.4 %all-gather.2.cloned.1.call-start = ((), (), s32[]{:S(2)}) async-start(), calls=%async_computation | async-start | bytes 8519680 | tf_op jit(solution)/shard_map/all_gather | solution.py:262
Sparse Core Ops, SparseCore 0:
  11.8 108.0 all-gather.1

commit v2 on v1

--- a/solution.py
+++ b/solution.py
@@ -14,6 +14,10 @@
 T = 128
 ROWS = 16
 PIECES = DK // ROWS
+NX = 4
+NY = 8
+HALF = 16
+START = (1, 3, 6, 8, 10, 10)
 F32 = jnp.float32
 BF16 = jnp.bfloat16
 
@@ -68,6 +72,7 @@
     og_ref,
     ig_ref,
     fg_ref,
+    w_ref,
     out_ref,
     part,
     recv,
@@ -83,23 +88,164 @@
     den_scr,
     sv_scr,
     gate_scr,
+    gated,
+    acc,
+    wa,
+    wb,
     send_sem,
     recv_sem,
+    wa_recv,
+    wb_recv,
+    w_send,
+    pair_send,
+    pair_recv,
 ):
     me = lax.axis_index("sp")
     size = lax.axis_size("sp")
     right = lax.rem(me + 1, size)
     left = lax.rem(me + size - 1, size)
 
+    place = lax.axis_index("dp")
+    core = lax.rem(place, 2)
+    x = lax.rem(lax.div(place, 2), NX)
+    y = lax.div(place, 2 * NX)
+
+    def wrap(a, n):
+        return lax.rem(a + n, n)
+
+    def device(xx, yy, cc):
+        return yy * (2 * NX) + xx * 2 + cc
+
+    x_up = device(wrap(x + 1, NX), y, core)
+    x_down = device(wrap(x - 1, NX), y, core)
+    y_up = device(x, wrap(y + 1, NY), core)
+    y_down = device(x, wrap(y - 1, NY), core)
+    pair = device(x, y, 1 - core)
+
     barrier = pltpu.get_barrier_semaphore()
     for other in (left, right):
         pl.semaphore_signal(barrier, inc=1, device_id={"sp": other}, device_id_type=MESH)
+    for other in (x_up, x_down, y_up, y_down, pair):
+        pl.semaphore_signal(barrier, inc=1, device_id={"dp": other}, device_id_type=MESH)
+
+    kinds = ((wa, wa_recv, 0), (wb, wb_recv, 1))
+
+    def slot(kind, xx, yy):
+        return yy * NX + xx if kind == 0 else xx * NY + yy
+
+    def block_send(kind, xx, yy, to, own=False):
+        buf, arrived, which = kinds[kind]
+        at = slot(kind, xx, yy)
+        src = w_ref.at[pl.ds(kind * HALF, HALF)] if own else buf.at[core, at]
+        pltpu.make_async_remote_copy(
+            src_ref=src,
+            dst_ref=buf.at[core, at],
+            send_sem=w_send.at[which],
+            recv_sem=arrived.at[at],
+            device_id={"dp": to},
+            device_id_type=MESH,
+        ).start()
+
+    def pair_copy(kind, xx, yy, own=False):
+        buf, _, which = kinds[kind]
+        at = slot(kind, xx, yy)
+        src = w_ref.at[pl.ds(kind * HALF, HALF)] if own else buf.at[core, at]
+        pltpu.make_async_remote_copy(
+            src_ref=src,
+            dst_ref=buf.at[core, at],
+            send_sem=pair_send.at[which],
+            recv_sem=pair_recv.at[which],
+            device_id={"dp": pair},
+            device_id_type=MESH,
+        ).start()
+
+    def block_wait(kind, xx, yy):
+        buf, arrived, which = kinds[kind]
+        at = slot(kind, xx, yy)
+        pltpu.make_async_remote_copy(
+            src_ref=buf.at[core, at],
+            dst_ref=buf.at[core, at],
+            send_sem=w_send.at[which],
+            recv_sem=arrived.at[at],
+            device_id={"dp": pair},
+            device_id_type=MESH,
+        ).wait_recv()
+
+    turn = 1 - 2 * core
+
+    def gather_own():
+        for kind in range(2):
+            for to in (x_up, x_down, y_up, y_down) if kind == 0 else (y_up, y_down, x_up, x_down):
+                block_send(kind, x, y, to, own=True)
+            pair_copy(kind, x, y, own=True)
+
+    def first_event(o, t):
+        xx, yy = wrap(x + o, NX), wrap(y - t, NY)
+        block_wait(0, xx, yy)
+        if t == 0 or t in (1, 2) or (t == 3 and o in (0, 1)):
+            block_send(0, xx, yy, y_up)
+        if t == 0 or t in (-1, -2) or (t == -3 and o in (-1, 2)):
+            block_send(0, xx, yy, y_down)
+        pair_copy(0, xx, yy)
+
+    def second_event(o, t):
+        xx, yy = wrap(x - o, NX), wrap(y - t, NY)
+        block_wait(1, xx, yy)
+        if o == 0 and t in (1, 2):
+            block_send(1, xx, yy, y_up)
+        if o == 0 and t in (-1, -2):
+            block_send(1, xx, yy, y_down)
+        if o == 0 or (o == 1 and t in (0, 1, 2, 3)):
+            block_send(1, xx, yy, x_up)
+        if o == 0 or (o == -1 and t not in (0, 1, 2, 3)):
+            block_send(1, xx, yy, x_down)
+        pair_copy(1, xx, yy)
+
+    def gather_round(hops):
+        for t in (0, 1, -1, 2, -2, 3, -3, 4):
+            for o in (0, 1, -1, 2):
+                if abs(o) + abs(t) == hops:
+                    first_event(o, t)
+                    if (o, t) == (-1, 0):
+                        block_send(
+                            0, wrap(x - turn, NX), y, device(wrap(x + turn, NX), y, core)
+                        )
+        for o in (0, 1, -1, 2):
+            for t in (0, 1, -1, 2, -2, 3, -3, 4):
+                if abs(o) + abs(t) == hops:
+                    second_event(o, t)
+                    if (o, t) == (0, -3):
+                        block_send(
+                            1, x, wrap(y - 3 * turn, NY), device(x, wrap(y + turn, NY), core)
+                        )
+
+    def gather_end():
+        for buf, _, which in kinds:
+            whole = pltpu.make_async_remote_copy(
+                src_ref=buf.at[core],
+                dst_ref=buf.at[1 - core],
+                send_sem=pair_send.at[which],
+                recv_sem=pair_recv.at[which],
+                device_id={"dp": pair},
+                device_id_type=MESH,
+            )
+            whole.wait_recv()
+            whole.wait_send()
+            sent = buf.at[core, pl.ds(0, NX * NY - 1)]
+            pltpu.make_async_remote_copy(
+                src_ref=sent,
+                dst_ref=sent,
+                send_sem=w_send.at[which],
+                recv_sem=pair_recv.at[which],
+                device_id={"dp": pair},
+                device_id_type=MESH,
+            ).wait_send()
 
     def piece_copy(i):
         return pltpu.make_async_remote_copy(
             src_ref=send.at[i],
             dst_ref=recv.at[i],
-            send_sem=send_sem.at[i],
+            send_sem=send_sem.at[0],
             recv_sem=recv_sem.at[i],
             device_id={"sp": right},
             device_id_type=MESH,
@@ -109,7 +255,7 @@
     head_copy = pltpu.make_async_remote_copy(
         src_ref=head_out,
         dst_ref=head_in,
-        send_sem=send_sem.at[last],
+        send_sem=send_sem.at[1],
         recv_sem=recv_sem.at[last],
         device_id={"sp": right},
         device_id_type=MESH,
@@ -125,7 +271,13 @@
     for h in range(HEADS):
         local_terms(h, q_ref, k_ref, v_ref, run, gain, part, norm_loc, top_loc, cm_scr, None)
 
-    pl.semaphore_wait(barrier, 2)
+    pl.semaphore_wait(barrier, 7)
+    @pl.when(me > 0)
+    def _():
+        gather_own()
+
+    wa[core, slot(0, x, y)] = w_ref[0:HALF, :]
+    wb[core, slot(1, x, y)] = w_ref[HALF:, :]
 
     def step_header(stab, norm):
         new = jnp.maximum(stab, top_loc[...])
@@ -150,6 +302,8 @@
                 return 0
 
             lax.fori_loop(0, PIECES, first, 0)
+
+        gather_own()
 
         def clear(i, _):
             recv[i] = jnp.zeros((ROWS, DV), BF16)
@@ -182,10 +336,33 @@
             cell = own * sv_scr[h, :, at] + old * carried[:, at]
             hidden = cell.astype(BF16).astype(F32)
             cols = slice(h * DV + c * T, h * DV + (c + 1) * T)
-            out_ref[:, cols] = (hidden * gate_scr[:, cols]).astype(BF16)
-
-    @pl.when(jnp.logical_and(me > 0, me < size - 1))
-    def _():
+            gated[:, at] = (hidden * gate_scr[:, cols]).astype(BF16)
+        ks = slice(h * DV, (h + 1) * DV)
+
+        def project(yy, _):
+            rows = []
+            for xx in range(NX):
+                for cc in range(2):
+                    rows.append(wa[cc, yy * NX + xx, :, ks])
+                    rows.append(wb[cc, xx * NY + yy, :, ks])
+            mine = lax.dot_general(
+                gated[...],
+                jnp.concatenate(rows, axis=0),
+                (((1,), (1,)), ((), ())),
+                preferred_element_type=F32,
+            )
+            if h > 0:
+                mine = mine + acc[yy]
+            if h < HEADS - 1:
+                acc[yy] = mine
+            else:
+                at = pl.ds(pl.multiple_of(yy * 2 * NX * 2 * HALF, 2 * NX * 2 * HALF), 2 * NX * 2 * HALF)
+                out_ref[:, at] = mine.astype(BF16)
+            return 0
+
+        lax.fori_loop(0, NY, project, 0)
+
+    def chain():
         head_copy.wait_recv()
         step_header(head_in[0:HEADS, :], head_in[HEADS:, :])
         head_copy.start()
@@ -201,6 +378,26 @@
 
             lax.fori_loop(0, PIECES, middle, 0)
 
+    ahead = jnp.int32(0)
+    for first_plane in START:
+        ahead = ahead + jnp.where(me >= first_plane, 1, 0)
+
+    def phase(p, _):
+        @pl.when(jnp.logical_and(p == ahead, jnp.logical_and(me > 0, me < size - 1)))
+        def _():
+            chain()
+
+        for hops in range(1, 7):
+
+            @pl.when(p == hops - 1)
+            def _(hops=hops):
+                gather_round(hops)
+
+        return 0
+
+    lax.fori_loop(0, 7, phase, 0)
+    gather_end()
+
     @pl.when(me == size - 1)
     def _():
         head_copy.wait_recv()
@@ -221,19 +418,22 @@
     def _():
         head_copy.wait_send()
 
-        def drain(i, _):
-            piece_copy(i).wait_send()
-            return 0
-
-        lax.fori_loop(0, last, drain, 0)
-
-
-def cell(q, k, v, og, ig, fg):
+        pltpu.make_async_remote_copy(
+            src_ref=send,
+            dst_ref=recv,
+            send_sem=send_sem.at[0],
+            recv_sem=recv_sem.at[last],
+            device_id={"sp": right},
+            device_id_type=MESH,
+        ).wait_send()
+
+
+def cell(q, k, v, og, ig, fg, w):
     pieces = HEADS * PIECES
     return pl.pallas_call(
         cell_kernel,
         out_shape=jax.ShapeDtypeStruct((T, HEADS * DV), BF16),
-        in_specs=[pl.BlockSpec(memory_space=pltpu.VMEM)] * 6,
+        in_specs=[pl.BlockSpec(memory_space=pltpu.VMEM)] * 7,
         out_specs=pl.BlockSpec(memory_space=pltpu.VMEM),
         scratch_shapes=[
             pltpu.VMEM((pieces, ROWS, DV), F32),
@@ -250,21 +450,33 @@
             pltpu.VMEM((HEADS, T, T), F32),
             pltpu.VMEM((HEADS, T, DV), F32),
             pltpu.VMEM((T, HEADS * DV), F32),
+            pltpu.VMEM((T, DV), BF16),
+            pltpu.VMEM((NY, T, 4 * NX * HALF), F32),
+            pltpu.VMEM((2, NX * NY, HALF, HEADS * DV), BF16),
+            pltpu.VMEM((2, NX * NY, HALF, HEADS * DV), BF16),
+            pltpu.SemaphoreType.DMA((2,)),
             pltpu.SemaphoreType.DMA((pieces + 1,)),
-            pltpu.SemaphoreType.DMA((pieces + 1,)),
+            pltpu.SemaphoreType.DMA((NX * NY,)),
+            pltpu.SemaphoreType.DMA((NX * NY,)),
+            pltpu.SemaphoreType.DMA((2,)),
+            pltpu.SemaphoreType.DMA((2,)),
+            pltpu.SemaphoreType.DMA((2,)),
         ],
         compiler_params=pltpu.CompilerParams(collective_id=0, has_side_effects=True),
         cost_estimate=pl.CostEstimate(flops=10**11, bytes_accessed=2 * 10**7, transcendentals=0),
-    )(q, k, v, og, ig, fg)
+    )(q, k, v, og, ig, fg, w)
 
 
 def body(queries, key_rows, values, out_gate, input_gate, forget_gate, out_weight):
-    whole_weight = lax.all_gather(out_weight, "dp", axis=1, tiled=True)
-    gated = cell(
-        queries[0], key_rows[0], values[0], out_gate[0], input_gate[0], forget_gate[0]
-    )
-    projected = jnp.dot(gated, whole_weight, preferred_element_type=F32)
-    return projected.astype(BF16)[None]
+    return cell(
+        queries[0],
+        key_rows[0],
+        values[0],
+        out_gate[0],
+        input_gate[0],
+        forget_gate[0],
+        out_weight.T,
+    )[None]
 
 
 def solution(mesh):

time: 134 us -> 81.5 us (0.61)
  the two profiles are of different devices: /device:TPU:1 before, /device:TPU:135 now
where the time goes in v2:
time: 81.5 us; the launch traced here: 81.3 us
  Pallas kernels  79.4 us (97%)
  local copies, waits for them, and re-layouts  1.88 us (2%)
    pallas_call x1, Pallas kernels, cell(): pl.pallas_call(cell_kernel, out_shape=jax.ShapeDtypeStruct((T, HEADS * DV...  79.4 us
    unnamed x1, local copies, waits for them, and re-layouts  1.88 us

profile of v2, /device:TPU:135, one launch (start us, length us, event | category | flops | bytes accessed | tf_op | source)
XLA Modules:
  0.0 81.3 jit_solution(14308591237896657758)
XLA Ops:
  0.0 79.4 %shard_map.73 = bf16[128,2048]{1,0:T(8,128)(2,1)} custom-call(bf16[128,1024]{1,0:T(8,128)(2,1)} %bitcast.11, bf16[128,1024]{1,0:T(8,128)(2,1)} %bitcast.12, bf16[128,2048]{1,0:T(8,128)(2,1)} %bitcast.9, bf16[128,2048]{1,0:T(8,128)(2,1)} %bitcast.10, bf16[4,128]{1,0:T(4,128)(2,1)} %bitcast.14, bf16[4,128]{1,0:T(4,128)(2,1)} %bitcast.15, bf16[32,2048]{1,0:T(8,128)(2,1)} %bitcast.13), custom_call_target="tpu_custom_call" | custom-call | flops 99999997952 | bytes 20000000 | tf_op jit(solution)/shard_map/pallas_call | solution.py:433
  79.4 1.9 %copy.9 = bf16[1,128,2048]{2,1,0:T(8,128)(2,1)} copy(bf16[1,128,2048]{2,1,0:T(8,128)(2,1)} %bitcast.8) | data formatting | bytes 1048576

commit v3 on v2

--- a/solution.py
+++ b/solution.py
@@ -17,7 +17,28 @@
 NX = 4
 NY = 8
 HALF = 16
-START = (1, 3, 6, 8, 10, 10)
+ORDER = (
+    (0, -1, 0), (0, 1, 0), (0, 0, -1), (0, 0, 1),
+    (1, 0, 1), (1, 1, 0), (1, 0, -1), (1, -1, 0),
+    (0, 2, 0), (0, -1, -1), (0, -1, 1), (1, -1, 1),
+    (1, 1, 1), (0, 1, -1), (0, 1, 1), (1, -1, -1),
+    (1, 2, 0), (0, 0, 2), (0, 0, -2), (1, 1, -1),
+    (1, 0, 2), (1, 0, -2), (0, 2, -1), (0, 2, 1),
+    (1, 2, 1), (1, 2, -1), (0, -1, 2), (0, -1, -2),
+    (1, -1, 2), (1, 1, 2), (0, 1, 2), (0, 1, -2),
+    (1, 1, -2), (1, -1, -2), (0, 0, -3), (0, 0, 3),
+    (1, 0, -3), (1, 0, 3), (1, 2, 2), (0, 2, -2),
+    (0, 2, 2), (1, 2, -2), (0, -1, -3), (0, -1, 3),
+    (1, 1, -3), (1, -1, -3), (0, 1, -3), (0, 1, 3),
+    (1, -1, 3), (1, 1, 3), (0, 0, 4), (0, 2, -3),
+    (1, 0, 4), (0, -1, 4), (1, 2, -3), (0, 2, 3),
+    (1, 2, 3), (0, 2, 4), (0, 1, 4), (1, 1, 4),
+    (1, -1, 4), (1, 2, 4),
+)
+ACROSS = ((0, 1, 0), (1, 0, 3))
+GROUP = 4
+GROUPS = -(-len(ORDER) // GROUP)
+SEGMENTS = 16
 F32 = jnp.float32
 BF16 = jnp.bfloat16
 
@@ -66,6 +87,14 @@
 
 
 def cell_kernel(
+    q_any,
+    k_any,
+    v_any,
+    og_any,
+    ig_any,
+    fg_any,
+    w_any,
+    out_ref,
     q_ref,
     k_ref,
     v_ref,
@@ -73,7 +102,6 @@
     ig_ref,
     fg_ref,
     w_ref,
-    out_ref,
     part,
     recv,
     send,
@@ -99,7 +127,24 @@
     w_send,
     pair_send,
     pair_recv,
+    load_sem,
 ):
+    loads = {
+        name: pltpu.make_async_copy(src, dst, load_sem.at[i])
+        for i, (name, src, dst) in enumerate(
+            (
+                ("fg", fg_any, fg_ref),
+                ("ig", ig_any, ig_ref),
+                ("k", k_any, k_ref),
+                ("v", v_any, v_ref),
+                ("w", w_any, w_ref),
+                ("q", q_any, q_ref),
+                ("og", og_any, og_ref),
+            )
+        )
+    }
+    for load in loads.values():
+        load.start()
     me = lax.axis_index("sp")
     size = lax.axis_size("sp")
     right = lax.rem(me + 1, size)
@@ -123,8 +168,15 @@
     pair = device(x, y, 1 - core)
 
     barrier = pltpu.get_barrier_semaphore()
-    for other in (left, right):
-        pl.semaphore_signal(barrier, inc=1, device_id={"sp": other}, device_id_type=MESH)
+
+    @pl.when(me > 0)
+    def _():
+        pl.semaphore_signal(barrier, inc=1, device_id={"sp": left}, device_id_type=MESH)
+
+    @pl.when(me < size - 1)
+    def _():
+        pl.semaphore_signal(barrier, inc=1, device_id={"sp": right}, device_id_type=MESH)
+
     for other in (x_up, x_down, y_up, y_down, pair):
         pl.semaphore_signal(barrier, inc=1, device_id={"dp": other}, device_id_type=MESH)
 
@@ -201,23 +253,16 @@
             block_send(1, xx, yy, x_down)
         pair_copy(1, xx, yy)
 
-    def gather_round(hops):
-        for t in (0, 1, -1, 2, -2, 3, -3, 4):
-            for o in (0, 1, -1, 2):
-                if abs(o) + abs(t) == hops:
-                    first_event(o, t)
-                    if (o, t) == (-1, 0):
-                        block_send(
-                            0, wrap(x - turn, NX), y, device(wrap(x + turn, NX), y, core)
-                        )
-        for o in (0, 1, -1, 2):
-            for t in (0, 1, -1, 2, -2, 3, -3, 4):
-                if abs(o) + abs(t) == hops:
-                    second_event(o, t)
-                    if (o, t) == (0, -3):
-                        block_send(
-                            1, x, wrap(y - 3 * turn, NY), device(x, wrap(y + turn, NY), core)
-                        )
+    def gather_group(events):
+        for kind, o, t in events:
+            if kind == 0:
+                first_event(o, t)
+            else:
+                second_event(o, t)
+            if (kind, o, t) == ACROSS[0]:
+                block_send(0, wrap(x - turn, NX), y, device(wrap(x + turn, NX), y, core))
+            if (kind, o, t) == ACROSS[1]:
+                block_send(1, x, wrap(y - 3 * turn, NY), device(x, wrap(y + turn, NY), core))
 
     def gather_end():
         for buf, _, which in kinds:
@@ -261,6 +306,8 @@
         device_id_type=MESH,
     )
 
+    for name in ("fg", "ig", "k", "v"):
+        loads[name].wait()
     gain = ig_ref[...].astype(F32)
     decay = -jnp.log1p(jnp.exp(-fg_ref[...].astype(F32)))
     row = lax.broadcasted_iota(jnp.int32, (T, T), 0)
@@ -271,7 +318,17 @@
     for h in range(HEADS):
         local_terms(h, q_ref, k_ref, v_ref, run, gain, part, norm_loc, top_loc, cm_scr, None)
 
-    pl.semaphore_wait(barrier, 7)
+    for name in ("w", "q", "og"):
+        loads[name].wait()
+    edge = jnp.logical_or(me == 0, me == size - 1)
+
+    @pl.when(edge)
+    def _():
+        pl.semaphore_wait(barrier, 6)
+
+    @pl.when(jnp.logical_not(edge))
+    def _():
+        pl.semaphore_wait(barrier, 7)
     @pl.when(me > 0)
     def _():
         gather_own()
@@ -346,8 +403,8 @@
                     rows.append(wa[cc, yy * NX + xx, :, ks])
                     rows.append(wb[cc, xx * NY + yy, :, ks])
             mine = lax.dot_general(
+                jnp.concatenate(rows, axis=0),
                 gated[...],
-                jnp.concatenate(rows, axis=0),
                 (((1,), (1,)), ((), ())),
                 preferred_element_type=F32,
             )
@@ -357,45 +414,52 @@
                 acc[yy] = mine
             else:
                 at = pl.ds(pl.multiple_of(yy * 2 * NX * 2 * HALF, 2 * NX * 2 * HALF), 2 * NX * 2 * HALF)
-                out_ref[:, at] = mine.astype(BF16)
+                out_ref[:, at] = jnp.transpose(mine).astype(BF16)
             return 0
 
         lax.fori_loop(0, NY, project, 0)
 
-    def chain():
-        head_copy.wait_recv()
-        step_header(head_in[0:HEADS, :], head_in[HEADS:, :])
-        head_copy.start()
-        for h in range(HEADS):
-
-            def middle(i, _, h=h):
-                at = h * PIECES + i
-                piece_copy(at).wait_recv()
-                new = keep_scr[h : h + 1, :] * recv[at].astype(F32) + add_scr[h : h + 1, :] * part[at]
-                send[at] = new.astype(BF16)
-                piece_copy(at).start()
-                return 0
-
-            lax.fori_loop(0, PIECES, middle, 0)
-
-    ahead = jnp.int32(0)
-    for first_plane in START:
-        ahead = ahead + jnp.where(me >= first_plane, 1, 0)
-
-    def phase(p, _):
-        @pl.when(jnp.logical_and(p == ahead, jnp.logical_and(me > 0, me < size - 1)))
+    def chain(segment):
+        @pl.when(segment == 0)
         def _():
-            chain()
-
-        for hops in range(1, 7):
-
-            @pl.when(p == hops - 1)
-            def _(hops=hops):
-                gather_round(hops)
-
-        return 0
-
-    lax.fori_loop(0, 7, phase, 0)
+            head_copy.wait_recv()
+            step_header(head_in[0:HEADS, :], head_in[HEADS:, :])
+            head_copy.start()
+
+        h = lax.div(segment * HEADS, SEGMENTS)
+        keep = keep_scr[pl.ds(h, 1), :]
+        add = add_scr[pl.ds(h, 1), :]
+
+        def middle(i, _):
+            at = segment * (last // SEGMENTS) + i
+            piece_copy(at).wait_recv()
+            send[at] = (keep * recv[at].astype(F32) + add * part[at]).astype(BF16)
+            piece_copy(at).start()
+            return 0
+
+        lax.fori_loop(0, last // SEGMENTS, middle, 0)
+
+    inner = jnp.logical_and(me > 0, me < size - 1)
+    begin = lax.div(4 * me + 2, 5)
+
+    def phase(p, done):
+        segment = p - begin
+        busy = jnp.logical_and(inner, jnp.logical_and(segment >= 0, segment < SEGMENTS))
+
+        @pl.when(busy)
+        def _():
+            chain(segment)
+
+        free = jnp.logical_or(jnp.logical_not(busy), lax.rem(p - begin + 64, 2) == 1)
+        for g in range(GROUPS):
+
+            @pl.when(jnp.logical_and(free, done == g))
+            def _(g=g):
+                gather_group(ORDER[g * GROUP : (g + 1) * GROUP])
+
+        return done + jnp.where(free, 1, 0)
+
+    lax.fori_loop(0, GROUPS + SEGMENTS // 2 + 4, phase, jnp.int32(0))
     gather_end()
 
     @pl.when(me == size - 1)
@@ -433,9 +497,10 @@
     return pl.pallas_call(
         cell_kernel,
         out_shape=jax.ShapeDtypeStruct((T, HEADS * DV), BF16),
-        in_specs=[pl.BlockSpec(memory_space=pltpu.VMEM)] * 7,
+        in_specs=[pl.BlockSpec(memory_space=pltpu.HBM)] * 7,
         out_specs=pl.BlockSpec(memory_space=pltpu.VMEM),
-        scratch_shapes=[
+        scratch_shapes=[pltpu.VMEM(a.shape, a.dtype) for a in (q, k, v, og, ig, fg, w)]
+        + [
             pltpu.VMEM((pieces, ROWS, DV), F32),
             pltpu.VMEM((pieces, ROWS, DV), BF16),
             pltpu.VMEM((pieces, ROWS, DV), BF16),
@@ -451,7 +516,7 @@
             pltpu.VMEM((HEADS, T, DV), F32),
             pltpu.VMEM((T, HEADS * DV), F32),
             pltpu.VMEM((T, DV), BF16),
-            pltpu.VMEM((NY, T, 4 * NX * HALF), F32),
+            pltpu.VMEM((NY, 4 * NX * HALF, T), F32),
             pltpu.VMEM((2, NX * NY, HALF, HEADS * DV), BF16),
             pltpu.VMEM((2, NX * NY, HALF, HEADS * DV), BF16),
             pltpu.SemaphoreType.DMA((2,)),
@@ -461,6 +526,7 @@
             pltpu.SemaphoreType.DMA((2,)),
             pltpu.SemaphoreType.DMA((2,)),
             pltpu.SemaphoreType.DMA((2,)),
+            pltpu.SemaphoreType.DMA((7,)),
         ],
         compiler_params=pltpu.CompilerParams(collective_id=0, has_side_effects=True),
         cost_estimate=pl.CostEstimate(flops=10**11, bytes_accessed=2 * 10**7, transcendentals=0),

time: 81.5 us -> 79.6 us (0.977)
  the two profiles are of different devices: /device:TPU:135 before, /device:TPU:902 now
where the time goes in v3:
time: 79.6 us; the launch traced here: 79.4 us
  Pallas kernels  77.5 us (97%)
  local copies, waits for them, and re-layouts  1.88 us (2%)
    pallas_call x1, Pallas kernels, cell(): pl.pallas_call(cell_kernel, out_shape=jax.ShapeDtypeStruct((T, HEADS * DV...  77.5 us
    unnamed x1, local copies, waits for them, and re-layouts  1.88 us

profile of v3, /device:TPU:902, one launch (start us, length us, event | category | flops | bytes accessed | tf_op | source)
XLA Modules:
  0.0 79.4 jit_solution(11516676599256201498)
XLA Ops:
  0.0 77.5 %shard_map.73 = bf16[128,2048]{1,0:T(8,128)(2,1)} custom-call(bf16[128,1024]{1,0:T(8,128)(2,1)} %bitcast.11, bf16[128,1024]{1,0:T(8,128)(2,1)} %bitcast.12, bf16[128,2048]{1,0:T(8,128)(2,1)} %bitcast.9, bf16[128,2048]{1,0:T(8,128)(2,1)} %bitcast.10, bf16[4,128]{1,0:T(4,128)(2,1)} %bitcast.14, bf16[4,128]{1,0:T(4,128)(2,1)} %bitcast.15, bf16[32,2048]{1,0:T(8,128)(2,1)} %bitcast.13), custom_call_target="tpu_custom_call" | custom-call | flops 99999997952 | bytes 20000000 | tf_op jit(solution)/shard_map/pallas_call | solution.py:497
  77.5 1.9 %copy.9 = bf16[1,128,2048]{2,1,0:T(8,128)(2,1)} copy(bf16[1,128,2048]{2,1,0:T(8,128)(2,1)} %bitcast.8) | data formatting | bytes 1048576
